TPU v7x, 32 devices: a whole 2x2x4 slice. The times are simulated.
32 devices in a mesh: sp: 8 (over z, x), tp: 4 (over y, core).
Axes of the slice: x: 2, y: 2, z: 4, core: 2. Of those that a mesh axis runs over, the one named last changes fastest.
Arguments:
- latent: bfloat16 [6144, 2048], P(('sp', 'tp')), may hold values from -6 to 6
- context: bfloat16 [1024, 2048], P('sp'), may hold values from -6 to 6
- conditioning: float32 [2, 2048], replicated, may hold values from -6 to 6
- norm_gain: float32 [2048], replicated, may hold values from 0.1 to 1.9
- mod_shift: bfloat16 [2048, 2048], P('sp', 'tp'), may hold values from -0.1875 to 0.1875
- mod_scale: bfloat16 [2048, 2048], P('sp', 'tp'), may hold values from -0.1875 to 0.1875
- mod_gate: bfloat16 [2048, 2048], P('sp', 'tp'), may hold values from -0.1875 to 0.1875
- w_query: bfloat16 [2048, 2048], P(None, 'tp'), may hold values from -4 to 4
- w_key: bfloat16 [2048, 2048], P(None, 'tp'), may hold values from -0.125 to 0.125
- w_value: bfloat16 [2048, 2048], P(None, 'tp'), may hold values from -0.125 to 0.125
- w_out: bfloat16 [2048, 2048], P('tp'), may hold values from -0.125 to 0.125
- lambdas: float32 [16], P('tp'), may hold values from 0.3 to 0.8
- context_bias: float32 [16], P('tp'), may hold values from 0.8 to 2.2
- head_gain: float32 [128], replicated, may hold values from 0.1 to 1.9
Outputs:
- updated: bfloat16 [6144, 2048], P(('sp', 'tp'))
All inputs are finite; a program needn't handle non-finite values.
Results may differ from a plain program's by a relative error of at most 0.01.
The roundings to bfloat16 on the way count: a program that leaves them out, or rounds other values in their place, can miss the bound.
Values may be sent and summed in bfloat16 or wider, within the bound.
A program may use at most 128 MiB of HBM per device.

v0:
```python
import jax
import jax.numpy as jnp
from jax import lax
from jax.sharding import PartitionSpec as P

EPS = 1e-06
NEGATIVE = -1e30


def modulated(inputs, norm_scale, offset_vec, scale_vec):
    rows_float = inputs.astype(jnp.float32)
    normal = rows_float * lax.rsqrt(jnp.mean(rows_float * rows_float, axis=-1, keepdims=True) + EPS)
    return (normal * norm_scale * (1.0 + scale_vec) + offset_vec).astype(jnp.bfloat16)


def block_size(length):
    for candidate in range(min(length, 1024), 0, -1):
        if length % candidate == 0:
            return candidate
    return length


def absorb(running, portion, context_flags, queries, bias_heads):
    head_count = queries.shape[1]
    head_dim = queries.shape[3]
    row_count = portion.shape[0]
    head_cols = head_count * 2 * head_dim
    key_rows = portion[:, :head_cols].reshape(row_count, head_count, 2, head_dim)
    value_rows = portion[:, head_cols:].reshape(row_count, head_count, 2 * head_dim)
    shifts = bias_heads[:, None, None] * context_flags[None, None, :]
    updated = []
    for which_map in range(2):
        previous, weight, accumulated = running[3 * which_map : 3 * which_map + 3]
        scores = (
            jnp.einsum(
                "qhd,khd->hqk",
                queries[:, :, which_map],
                key_rows[:, :, which_map],
                preferred_element_type=jnp.float32,
            )
            * head_dim ** (-0.5)
            + shifts
        )
        peak_new = jnp.maximum(previous, jnp.max(scores, axis=2))
        faded = jnp.exp(previous - peak_new)
        raised = jnp.exp(scores - peak_new[:, :, None])
        weight = weight * faded + jnp.sum(raised, axis=2)
        accumulated = accumulated * faded.T[:, :, None] + jnp.einsum(
            "hqk,khd->qhd",
            raised.astype(jnp.bfloat16),
            value_rows,
            preferred_element_type=jnp.float32,
        )
        updated += [peak_new, weight, accumulated]
    return tuple(updated)


def absorb_rows(running, portion, context_flags, queries, bias_heads):
    row_count = portion.shape[0]
    block_len = block_size(row_count)
    if block_len == row_count:
        return absorb(running, portion, context_flags, queries, bias_heads)
    stacked = portion.reshape(row_count // block_len, block_len, portion.shape[1])
    flag_blocks = context_flags.reshape(row_count // block_len, block_len)

    def advance(state_now, operand):
        return (absorb(state_now, operand[0], operand[1], queries, bias_heads), None)

    running, unused = lax.scan(advance, running, (stacked, flag_blocks))
    return running


def per_device(
    latent,
    context,
    conditioning,
    norm_gain,
    mod_shift,
    mod_scale,
    mod_gate,
    w_query,
    w_key,
    w_value,
    w_out,
    lambdas,
    context_bias,
    head_gain,
):
    head_dim = head_gain.shape[0] // 2
    head_count = lambdas.shape[0]
    rows_sp = mod_shift.shape[0]
    cond_rows = lax.dynamic_slice_in_dim(conditioning, lax.axis_index("sp") * rows_sp, rows_sp, 1)
    activated = jax.nn.silu(cond_rows).astype(jnp.bfloat16)
    partials = jnp.stack(
        [
            jnp.dot(activated, matrix, preferred_element_type=jnp.float32)
            for matrix in (mod_shift, mod_scale, mod_gate)
        ],
        axis=1,
    )
    summed = lax.psum(partials, "sp")
    modulation = lax.all_gather(summed, "tp", axis=2, tiled=True)
    own_rows = modulated(latent, norm_gain, modulation[0, 0], modulation[0, 1])
    context_rows = modulated(context, norm_gain, modulation[1, 0], modulation[1, 1])
    key_value = jnp.concatenate([w_key, w_value], axis=1)
    projector = jnp.concatenate([w_query, key_value], axis=1)
    projected = jnp.dot(
        lax.all_gather(own_rows, "tp", axis=0, tiled=True),
        projector,
        preferred_element_type=jnp.float32,
    ).astype(jnp.bfloat16)
    head_cols = w_query.shape[1]
    token_count = projected.shape[0]
    queries = projected[:, :head_cols].reshape(token_count, head_count, 2, head_dim)
    latent_kv = projected[:, head_cols:]
    context_kv = jnp.dot(context_rows, key_value, preferred_element_type=jnp.float32).astype(
        jnp.bfloat16
    )
    first_map = (
        jnp.full((head_count, token_count), NEGATIVE, jnp.float32),
        jnp.zeros((head_count, token_count), jnp.float32),
        jnp.zeros((token_count, head_count, 2 * head_dim), jnp.float32),
    )
    initial = first_map + first_map
    every_context = lax.all_gather(context_kv, "sp", axis=0, tiled=True)
    running = absorb_rows(
        initial,
        every_context,
        jnp.ones((every_context.shape[0],), jnp.float32),
        queries,
        context_bias,
    )
    portion = lax.all_gather(latent_kv, "sp", axis=0, tiled=True)
    running = absorb_rows(
        running, portion, jnp.zeros((portion.shape[0],), jnp.float32), queries, context_bias
    )
    peak_one, total_one, accum_one, peak_two, total_two, accum_two = running
    mixed = accum_one / total_one.T[:, :, None] - lambdas[None, :, None] * (
        accum_two / total_two.T[:, :, None]
    )
    normed = mixed * lax.rsqrt(jnp.mean(mixed * mixed, axis=-1, keepdims=True) + EPS) * head_gain
    flattened = normed.reshape(token_count, head_cols).astype(jnp.bfloat16)
    attended = lax.psum_scatter(
        jnp.dot(flattened, w_out, preferred_element_type=jnp.float32).astype(jnp.bfloat16),
        "tp",
        scatter_dimension=0,
        tiled=True,
    )
    return (latent.astype(jnp.float32) + modulation[0, 2] * attended.astype(jnp.float32)).astype(
        jnp.bfloat16
    )


def solution(mesh):
    return jax.shard_map(
        per_device,
        mesh=mesh,
        in_specs=(
            P(("sp", "tp"), None),
            P("sp", None),
            P(),
            P(),
            P("sp", "tp"),
            P("sp", "tp"),
            P("sp", "tp"),
            P(None, "tp"),
            P(None, "tp"),
            P(None, "tp"),
            P("tp", None),
            P("tp"),
            P("tp"),
            P(),
        ),
        out_specs=P(("sp", "tp"), None),
        check_vma=False,
    )
```

profile of v0, /device:TPU:0, one launch (start us, length us, event | category | flops | bytes accessed | tf_op | source)
XLA Modules:
  0.0 557.7 jit_solution(13907041467783386179)
XLA Ops:
  10.0 38.8 %psum.7 = f32[2,3,512]{2,0,1:T(2,128)S(1)} all-reduce(f32[2,3,512]{2,0,1:T(2,128)S(1)} %pad_maximum_fusion), channel_id=1, replica_groups=mesh['sp'=8,'tp'=4] {'sp'}, use_global_device_ids=true, to_apply=%region_0.1 | all-reduce | flops 3072 | bytes 24576 | tf_op jit(solution)/shard_map/psum | solution.py:101
  48.9 5.2 all_gather.12
  59.8 4.0 fusion.57
  63.9 20.6 %all-gather.4.cloned.1.call-done = bf16[768,2048]{1,0:T(8,128)(2,1)} async-done(((bf16[192,2048]{1,0:T(8,128)(2,1)}), bf16[768,2048]{1,0:T(8,128)(2,1)}) %all-gather.4.cloned.1.call-update) | async-done | bytes 3145744 | tf_op jit(solution)/shard_map/all_gather | solution.py:108
  84.5 8.8 %fusion.44 = bf16[768,1536]{1,0:T(8,128)(2,1)S(1)} fusion(bf16[768,2048]{1,0:T(8,128)(2,1)} %all-gather.4.cloned.1.call-done, bf16[2048,512]{1,0:T(8,128)(2,1)} %param.25, bf16[2048,512]{1,0:T(8,128)(2,1)} %param.24, bf16[2048,512]{1,0:T(8,128)(2,1)} %param.23), kind=kOutput, calls=%fused_computation.56 | convolution fusion | flops 4851892224 | bytes 11796480 | tf_op jit(solution)/shard_map/dot_general | solution.py:107
  96.4 39.3 %all-gather.6.cloned.1.call-done = bf16[1024,1024]{1,0:T(8,128)(2,1)} async-done(((bf16[128,1024]{1,0:T(8,128)(2,1)}), bf16[1024,1024]{1,0:T(8,128)(2,1)}) %all-gather.6.cloned.1.call-update) | async-done | bytes 2097168 | tf_op jit(solution)/shard_map/all_gather | solution.py:125
  135.7 2.7 fusion.85
  146.5 3.1 fusion.67
  149.7 6.2 %fusion.25 = (f32[4,768]{1,0:T(4,128)S(1)}, f32[4,768]{1,0:T(4,128)S(1)}, f32[4,768,1024]{2,1,0:T(8,128)}) fusion(f32[4]{0:T(128)S(1)} %copy-done.9, f32[4,768,1024]{2,1,0:T(8,128)S(1)} %fusion.67, bf16[1024,4,2,64]{0,3,2,1:T(8,128)(2,1)S(1)} %bitcast.155, bf16[768,4,2,64]{0,3,2,1:T(8,128)(2,1)S(1)} %bitcast.153), kind=kOutput, calls=%fused_computation.39 | convolution fusion | flops 421521408 | bytes 26108416 | tf_op jit(solution)/shard_map/qhd,khd->hqk/dot_general | solution.py:35
  155.8 8.2 %fusion.29 = (f32[4,768]{1,0:T(4,128)S(1)}, f32[4,768]{1,0:T(4,128)S(1)}) fusion(f32[4,768,1024]{2,1,0:T(8,128)} %get-tuple-element.134, f32[4,768]{1,0:T(4,128)S(1)} %broadcast_maximum_fusion, f32[4]{0:T(128)S(1)} %copy-done.9, f32[4,768]{1,0:T(4,128)S(1)} %broadcast_maximum_fusion.1, f32[4,768,1024]{2,1,0:T(8,128)S(1)} %fusion.67), kind=kLoop, calls=%fused_computation.43 | loop fusion | flops 25159680 | bytes 25214992 | tf_op jit(solution)/shard_map/reduce_sum | solution.py:47
  164.0 8.6 %bitcast_add_fusion.2 = f32[768,4,128]{0,2,1:T(8,128)} fusion(bf16[1024,4,128]{0,2,1:T(8,128)(2,1)S(1)} %bitcast.156, f32[4,768,1024]{2,1,0:T(8,128)} %get-tuple-element.134, f32[4,768]{1,0:T(4,128)S(1)} %broadcast_maximum_fusion, f32[4]{0:T(128)S(1)} %copy-done.9, f32[768,4]{0,1:T(4,128)S(1)} %get-tuple-element.136), kind=kOutput, calls=%fused_computation.67 | convolution fusion | flops 818282496 | bytes 15228944 | tf_op jit(solution)/shard_map/hqk,khd->qhd/dot_general | solution.py:48
  172.7 4.1 bitcast_add_fusion.3
  176.8 135.7 %all-gather.8.cloned.1.call-done = bf16[6144,1024]{1,0:T(8,128)(2,1)} async-done(((bf16[768,1024]{1,0:T(8,128)(2,1)}), bf16[6144,1024]{1,0:T(8,128)(2,1)}) %all-gather.8.cloned.1.call-update) | async-done | bytes 12582928 | tf_op jit(solution)/shard_map/all_gather | solution.py:133
  312.6 193.9 %while.20 = (s32[]{:T(128)}, f32[4,768]{1,0:T(4,128)S(1)}, f32[4,768]{1,0:T(4,128)S(1)}, f32[768,4,128]{0,2,1:T(8,128)}, f32[4,768]{1,0:T(4,128)S(1)}, /*index=5...) while((s32[]{:T(128)}, f32[4,768]{1,0:T(4,128)S(1)}, ...), condition=%wide.region_12.13_spmd, body=%wide.region_7.12_spmd.sunk | while | flops 2486716416 | bytes 128058136 | solution.py:69
  312.6 3.1 constant_dynamic-slice_fusion.2
  315.7 3.9 copy.54
  319.6 2.7 fusion.114
  322.3 2.8 fusion.115
  325.1 5.5 bitcast_reduce_fusion.3
  330.7 5.8 %bitcast_add_fusion.7 = f32[768,4,128]{0,2,1:T(8,128)} fusion(f32[768,4,128]{0,2,1:T(8,128)} %get-tuple-element.241, bf16[1024,4,128]{0,2,1:T(8,128)(2,1)} %bitcast.148, f32[4,1024,768]{2,1,0:T(8,128)S(1)} %get-tuple-element.214, f32[4,768]{1,0:T(4,128)S(1)} %get-tuple-element.250, f32[4]{0:T(128)S(1)} %broadcast_multiply_fusion.2, ...), kind=kOutput, calls=%fused_computation.14.clone.1 | convolution fusion | flops 818675712 | bytes 16801808 | tf_op jit(solution)/shard_map/while/body/eval_jaxpr/hqk,khd->qhd/dot_general | solution.py:48
  336.5 3.2 bitcast_add_fusion.6
  339.7 5.1 fusion.118
  344.9 3.1 constant_dynamic-slice_fusion.2
  348.0 3.9 copy.54
  351.9 2.7 fusion.114
  354.6 2.8 fusion.115
  357.5 5.5 bitcast_reduce_fusion.3
  363.0 5.8 %bitcast_add_fusion.7 = f32[768,4,128]{0,2,1:T(8,128)} fusion(f32[768,4,128]{0,2,1:T(8,128)} %get-tuple-element.241, bf16[1024,4,128]{0,2,1:T(8,128)(2,1)} %bitcast.148, f32[4,1024,768]{2,1,0:T(8,128)S(1)} %get-tuple-element.214, f32[4,768]{1,0:T(4,128)S(1)} %get-tuple-element.250, f32[4]{0:T(128)S(1)} %broadcast_multiply_fusion.2, ...), kind=kOutput, calls=%fused_computation.14.clone.1 | convolution fusion | flops 818675712 | bytes 16801808 | tf_op jit(solution)/shard_map/while/body/eval_jaxpr/hqk,khd->qhd/dot_general | solution.py:48
  368.8 3.2 bitcast_add_fusion.6
  372.0 5.1 fusion.118
  377.2 3.1 constant_dynamic-slice_fusion.2
  380.3 3.9 copy.54
  384.2 2.7 fusion.114
  386.9 2.8 fusion.115
  389.8 5.5 bitcast_reduce_fusion.3
  395.3 5.8 %bitcast_add_fusion.7 = f32[768,4,128]{0,2,1:T(8,128)} fusion(f32[768,4,128]{0,2,1:T(8,128)} %get-tuple-element.241, bf16[1024,4,128]{0,2,1:T(8,128)(2,1)} %bitcast.148, f32[4,1024,768]{2,1,0:T(8,128)S(1)} %get-tuple-element.214, f32[4,768]{1,0:T(4,128)S(1)} %get-tuple-element.250, f32[4]{0:T(128)S(1)} %broadcast_multiply_fusion.2, ...), kind=kOutput, calls=%fused_computation.14.clone.1 | convolution fusion | flops 818675712 | bytes 16801808 | tf_op jit(solution)/shard_map/while/body/eval_jaxpr/hqk,khd->qhd/dot_general | solution.py:48
  401.1 3.2 bitcast_add_fusion.6
  404.3 5.1 fusion.118
  409.5 3.1 constant_dynamic-slice_fusion.2
  412.6 3.9 copy.54
  416.6 2.7 fusion.114
  419.3 2.8 fusion.115
  422.1 5.5 bitcast_reduce_fusion.3
  427.6 5.8 %bitcast_add_fusion.7 = f32[768,4,128]{0,2,1:T(8,128)} fusion(f32[768,4,128]{0,2,1:T(8,128)} %get-tuple-element.241, bf16[1024,4,128]{0,2,1:T(8,128)(2,1)} %bitcast.148, f32[4,1024,768]{2,1,0:T(8,128)S(1)} %get-tuple-element.214, f32[4,768]{1,0:T(4,128)S(1)} %get-tuple-element.250, f32[4]{0:T(128)S(1)} %broadcast_multiply_fusion.2, ...), kind=kOutput, calls=%fused_computation.14.clone.1 | convolution fusion | flops 818675712 | bytes 16801808 | tf_op jit(solution)/shard_map/while/body/eval_jaxpr/hqk,khd->qhd/dot_general | solution.py:48
  433.4 3.2 bitcast_add_fusion.6
  436.6 5.1 fusion.118
  441.9 3.1 constant_dynamic-slice_fusion.2
  445.0 3.9 copy.54
  448.9 2.7 fusion.114
  451.6 2.8 fusion.115
  454.4 5.5 bitcast_reduce_fusion.3
  459.9 5.8 %bitcast_add_fusion.7 = f32[768,4,128]{0,2,1:T(8,128)} fusion(f32[768,4,128]{0,2,1:T(8,128)} %get-tuple-element.241, bf16[1024,4,128]{0,2,1:T(8,128)(2,1)} %bitcast.148, f32[4,1024,768]{2,1,0:T(8,128)S(1)} %get-tuple-element.214, f32[4,768]{1,0:T(4,128)S(1)} %get-tuple-element.250, f32[4]{0:T(128)S(1)} %broadcast_multiply_fusion.2, ...), kind=kOutput, calls=%fused_computation.14.clone.1 | convolution fusion | flops 818675712 | bytes 16801808 | tf_op jit(solution)/shard_map/while/body/eval_jaxpr/hqk,khd->qhd/dot_general | solution.py:48
  465.7 3.2 bitcast_add_fusion.6
  469.0 5.1 fusion.118
  474.2 3.1 constant_dynamic-slice_fusion.2
  477.3 3.9 copy.54
  481.2 2.7 fusion.114
  483.9 2.8 fusion.115
  486.7 5.5 bitcast_reduce_fusion.3
  492.3 5.8 %bitcast_add_fusion.7 = f32[768,4,128]{0,2,1:T(8,128)} fusion(f32[768,4,128]{0,2,1:T(8,128)} %get-tuple-element.241, bf16[1024,4,128]{0,2,1:T(8,128)(2,1)} %bitcast.148, f32[4,1024,768]{2,1,0:T(8,128)S(1)} %get-tuple-element.214, f32[4,768]{1,0:T(4,128)S(1)} %get-tuple-element.250, f32[4]{0:T(128)S(1)} %broadcast_multiply_fusion.2, ...), kind=kOutput, calls=%fused_computation.14.clone.1 | convolution fusion | flops 818675712 | bytes 16801808 | tf_op jit(solution)/shard_map/while/body/eval_jaxpr/hqk,khd->qhd/dot_general | solution.py:48
  498.1 3.2 bitcast_add_fusion.6
  501.3 5.1 fusion.118
  509.1 3.5 convolution_convert_fusion
  512.7 36.2 %reduce-scatter.2.cloned.1.call-done = bf16[192,2048]{1,0:T(8,128)(2,1)} async-done(((bf16[768,2048]{1,0:T(8,128)(2,1)}), bf16[192,2048]{1,0:T(8,128)(2,1)}) %reduce-scatter.2.cloned.1.call-update) | async-done | bytes 786448 | tf_op jit(solution)/shard_map/reduce_scatter | solution.py:143
  (121 shorter events, 26.0 us)
Async XLA Ops:
  6.5 502.6 %copy-start = (bf16[512,2048]{1,0:T(8,128)(2,1)S(1)}, bf16[512,2048]{1,0:T(8,128)(2,1)}, u32[]{:S(2)}) copy-start(bf16[512,2048]{1,0:T(8,128)(2,1)} %param.26) | copy-start | bytes 6291460
  6.5 77.9 %all-gather.4.cloned.1.call-start = ((), (), s32[]{:S(2)}) async-start(), calls=%async_computation.1 | async-start | bytes 3932160 | tf_op jit(solution)/shard_map/all_gather | solution.py:108
  58.5 77.2 %all-gather.6.cloned.1.call-start = ((), (), s32[]{:S(2)}) async-start(), calls=%async_computation.2 | async-start | bytes 2359296 | tf_op jit(solution)/shard_map/all_gather | solution.py:125
  63.8 248.7 %all-gather.8.cloned.1.call-start = ((), (), s32[]{:S(2)}) async-start(), calls=%async_computation.3 | async-start | bytes 14155776 | tf_op jit(solution)/shard_map/all_gather | solution.py:133
  93.2 1.4 copy-start.4
  96.2 452.7 %reduce-scatter.2.cloned.1.call-start = ((), (), s32[]{:S(2)}) async-start(), calls=%async_computation.4 | async-start | bytes 3932160 | tf_op jit(solution)/shard_map/reduce_scatter | solution.py:143
  146.5 3.1 copy-start.3
  146.5 3.1 copy-start.9
  155.8 8.2 %copy-start.7 = (bf16[1024,512]{0,1:T(8,128)(2,1)S(1)}, bf16[1024,512]{0,1:T(8,128)(2,1)}, u32[]{:S(2)}) copy-start(bf16[1024,512]{0,1:T(8,128)(2,1)} %copy.41) | copy-start | bytes 3145732
  312.6 193.9 %copy-start.10 = (f32[4]{0:T(128)S(1)}, f32[4]{0:T(128)}, u32[]{:S(2)}) copy-start(f32[4]{0:T(128)} %param.27) | copy-start | bytes 52
  312.6 196.2 %copy-start.11 = (f32[128]{0:T(128)S(1)}, f32[128]{0:T(128)}, u32[]{:S(2)}) copy-start(f32[128]{0:T(128)} %param.29) | copy-start | bytes 1540
  330.6 5.8 %copy-start.1 = (bf16[1024,512]{0,1:T(8,128)(2,1)S(1)}, bf16[1024,512]{0,1:T(8,128)(2,1)}, u32[]{:S(2)}) copy-start(bf16[1024,512]{0,1:T(8,128)(2,1)} %get-tuple-element.220) | copy-start | bytes 3145732 | tf_op jit(solution)/shard_map/while
  330.6 5.8 %copy-start.5 = (f32[768,4,128]{0,2,1:T(8,128)S(1)}, f32[768,4,128]{0,2,1:T(8,128)}, u32[]{:S(2)}) copy-start(f32[768,4,128]{0,2,1:T(8,128)} %get-tuple-element.238) | copy-start | bytes 4718596 | tf_op jit(solution)/shard_map/while
  339.7 5.2 copy-start.6
  363.0 5.8 %copy-start.1 = (bf16[1024,512]{0,1:T(8,128)(2,1)S(1)}, bf16[1024,512]{0,1:T(8,128)(2,1)}, u32[]{:S(2)}) copy-start(bf16[1024,512]{0,1:T(8,128)(2,1)} %get-tuple-element.220) | copy-start | bytes 3145732 | tf_op jit(solution)/shard_map/while
  363.0 5.8 %copy-start.5 = (f32[768,4,128]{0,2,1:T(8,128)S(1)}, f32[768,4,128]{0,2,1:T(8,128)}, u32[]{:S(2)}) copy-start(f32[768,4,128]{0,2,1:T(8,128)} %get-tuple-element.238) | copy-start | bytes 4718596 | tf_op jit(solution)/shard_map/while
  372.0 5.2 copy-start.6
  395.3 5.8 %copy-start.1 = (bf16[1024,512]{0,1:T(8,128)(2,1)S(1)}, bf16[1024,512]{0,1:T(8,128)(2,1)}, u32[]{:S(2)}) copy-start(bf16[1024,512]{0,1:T(8,128)(2,1)} %get-tuple-element.220) | copy-start | bytes 3145732 | tf_op jit(solution)/shard_map/while
  395.3 5.8 %copy-start.5 = (f32[768,4,128]{0,2,1:T(8,128)S(1)}, f32[768,4,128]{0,2,1:T(8,128)}, u32[]{:S(2)}) copy-start(f32[768,4,128]{0,2,1:T(8,128)} %get-tuple-element.238) | copy-start | bytes 4718596 | tf_op jit(solution)/shard_map/while
  404.3 5.2 copy-start.6
  427.6 5.8 %copy-start.1 = (bf16[1024,512]{0,1:T(8,128)(2,1)S(1)}, bf16[1024,512]{0,1:T(8,128)(2,1)}, u32[]{:S(2)}) copy-start(bf16[1024,512]{0,1:T(8,128)(2,1)} %get-tuple-element.220) | copy-start | bytes 3145732 | tf_op jit(solution)/shard_map/while
  427.6 5.8 %copy-start.5 = (f32[768,4,128]{0,2,1:T(8,128)S(1)}, f32[768,4,128]{0,2,1:T(8,128)}, u32[]{:S(2)}) copy-start(f32[768,4,128]{0,2,1:T(8,128)} %get-tuple-element.238) | copy-start | bytes 4718596 | tf_op jit(solution)/shard_map/while
  436.6 5.2 copy-start.6
  459.9 5.8 %copy-start.1 = (bf16[1024,512]{0,1:T(8,128)(2,1)S(1)}, bf16[1024,512]{0,1:T(8,128)(2,1)}, u32[]{:S(2)}) copy-start(bf16[1024,512]{0,1:T(8,128)(2,1)} %get-tuple-element.220) | copy-start | bytes 3145732 | tf_op jit(solution)/shard_map/while
  459.9 5.8 %copy-start.5 = (f32[768,4,128]{0,2,1:T(8,128)S(1)}, f32[768,4,128]{0,2,1:T(8,128)}, u32[]{:S(2)}) copy-start(f32[768,4,128]{0,2,1:T(8,128)} %get-tuple-element.238) | copy-start | bytes 4718596 | tf_op jit(solution)/shard_map/while
  468.9 5.2 copy-start.6
  492.2 5.8 %copy-start.1 = (bf16[1024,512]{0,1:T(8,128)(2,1)S(1)}, bf16[1024,512]{0,1:T(8,128)(2,1)}, u32[]{:S(2)}) copy-start(bf16[1024,512]{0,1:T(8,128)(2,1)} %get-tuple-element.220) | copy-start | bytes 3145732 | tf_op jit(solution)/shard_map/while
  492.2 5.8 %copy-start.5 = (f32[768,4,128]{0,2,1:T(8,128)S(1)}, f32[768,4,128]{0,2,1:T(8,128)}, u32[]{:S(2)}) copy-start(f32[768,4,128]{0,2,1:T(8,128)} %get-tuple-element.238) | copy-start | bytes 4718596 | tf_op jit(solution)/shard_map/while
  501.3 5.2 copy-start.6
  509.1 39.8 %copy-start.2 = (bf16[192,2048]{1,0:T(8,128)(2,1)S(1)}, bf16[192,2048]{1,0:T(8,128)(2,1)}, u32[]{:S(2)}) copy-start(bf16[192,2048]{1,0:T(8,128)(2,1)} %param.16) | copy-start | bytes 2359300
  509.1 39.8 %copy-start.8 = (f32[1,1,2048]{2,0,1:T(1,128)S(1)}, f32[1,1,2048]{2,0,1:T(1,128)}, u32[]{:S(2)}) copy-start(f32[1,1,2048]{2,0,1:T(1,128)} %get-tuple-element.125) | copy-start | bytes 24580
Sparse Core Ops, SparseCore 0:
  58.6 25.7 all-gather.3
  86.6 49.0 all-gather.5
  137.9 174.6 all-gather.7
  512.8 36.0 reduce-scatter.1
where the time goes:
time: 559 us; the launch traced here: 558 us
  waiting for transfers between devices  232 us (42%)
  matrix products  145 us (26%)
  local copies, waits for them, and re-layouts  72.2 us (13%)
  other arithmetic  49.9 us (9%)
  blocking collectives  44 us (8%)
  between operations  13.3 us (2%)
    all_gather x1, waiting for transfers between devices, per_device(): portion = lax.all_gather(latent_kv, 'sp', axis=0, tiled=True)  136 us
    dot_general x14, matrix products, absorb(): jnp.einsum('hqk,khd->qhd', raised.astype(jnp.bfloat16), value_rows, prefe...  66.5 us
    dot_general x14, matrix products, absorb(): jnp.einsum('qhd,khd->hqk', queries[:, :, which_map], key_rows[:, :, which...  59 us
    dynamic_slice x12, local copies, waits for them, and re-layouts, absorb_rows(): running, unused = lax.scan(advance, running, (stacked, flag_blocks))  42.2 us
    all_gather x1, waiting for transfers between devices, per_device(): every_context = lax.all_gather(context_kv, 'sp', axis=0, tiled=True)  39.3 us
    reduce_sum x7, other arithmetic, absorb(): weight = weight * faded + jnp.sum(raised, axis=2)  39 us
    psum x1, blocking collectives, per_device(): summed = lax.psum(partials, 'sp')  38.8 us
    reduce_scatter x1, waiting for transfers between devices, per_device(): lax.psum_scatter(jnp.dot(flattened, w_out, preferred_element_type=jnp.flo...  36.2 us
  transfers between devices with their start and end apart: 4, of which 4 were waited for; matrix products, arithmetic and copies ran while one was open for 10% of the time, Pallas kernels for 0%

commit v1 on v0

--- a/solution.py
+++ b/solution.py
@@ -98,7 +98,9 @@
         ],
         axis=1,
     )
-    summed = lax.psum(partials, "sp")
+    summed = partials
+    for hop in (1, 2, 4):
+        summed = summed + lax.ppermute(summed, "sp", [(dev, dev ^ hop) for dev in range(8)])
     modulation = lax.all_gather(summed, "tp", axis=2, tiled=True)
     own_rows = modulated(latent, norm_gain, modulation[0, 0], modulation[0, 1])
     context_rows = modulated(context, norm_gain, modulation[1, 0], modulation[1, 1])

time: 559 us -> 537 us (0.961)
  blocking collectives: 44 us -> 5.22 us
  starting transfers between devices: 0.31 us -> 8.61 us
  waiting for transfers between devices: 232 us -> 240 us
    psum x1 -> x0, blocking collectives: 38.8 us -> none  [per_device(): summed = lax.psum(partials, 'sp')]
    ppermute x0 -> x3, starting transfers between devices: none -> 8.3 us  [per_device(): lax.ppermute(summed, 'sp', [(dev, dev ^ hop) for dev in range(8)])]
  transfers between devices with their start and end apart: 4 -> 7, of which waited for: 4 -> 7; matrix products, arithmetic and copies ran while one was open for 10% -> 11% of each run, Pallas kernels for 0% -> 0%
where the time goes in v1:
time: 537 us; the launch traced here: 535 us
  waiting for transfers between devices  240 us (45%)
  matrix products  145 us (27%)
  local copies, waits for them, and re-layouts  72.1 us (13%)
  other arithmetic  49.9 us (9%)
  between operations  13.3 us (2%)
  starting transfers between devices  8.61 us (2%)
    all_gather x1, waiting for transfers between devices, per_device(): portion = lax.all_gather(latent_kv, 'sp', axis=0, tiled=True)  136 us
    dot_general x14, matrix products, absorb(): jnp.einsum('hqk,khd->qhd', raised.astype(jnp.bfloat16), value_rows, prefe...  66.5 us
    dot_general x14, matrix products, absorb(): jnp.einsum('qhd,khd->hqk', queries[:, :, which_map], key_rows[:, :, which...  59 us
    dynamic_slice x12, local copies, waits for them, and re-layouts, absorb_rows(): running, unused = lax.scan(advance, running, (stacked, flag_blocks))  42 us
    all_gather x1, waiting for transfers between devices, per_device(): every_context = lax.all_gather(context_kv, 'sp', axis=0, tiled=True)  39.3 us
    reduce_sum x7, other arithmetic, absorb(): weight = weight * faded + jnp.sum(raised, axis=2)  39 us
    reduce_scatter x1, waiting for transfers between devices, per_device(): lax.psum_scatter(jnp.dot(flattened, w_out, preferred_element_type=jnp.flo...  36.2 us
    all_gather x1, waiting for transfers between devices, per_device(): lax.all_gather(own_rows, 'tp', axis=0, tiled=True)  25 us
  transfers between devices with their start and end apart: 7, of which 7 were waited for; matrix products, arithmetic and copies ran while one was open for 11% of the time, Pallas kernels for 0%

profile of v1, /device:TPU:0, one launch (start us, length us, event | category | flops | bytes accessed | tf_op | source)
XLA Modules:
  0.0 535.1 jit_solution(4041627896141865876)
XLA Ops:
  10.0 3.0 collective-permute-start
  18.6 3.1 collective-permute-start.2
  23.4 5.2 all_gather.12
  33.0 3.9 fusion.57
  36.9 25.0 %all-gather.4.cloned.1.call-done = bf16[768,2048]{1,0:T(8,128)(2,1)} async-done(((bf16[192,2048]{1,0:T(8,128)(2,1)}), bf16[768,2048]{1,0:T(8,128)(2,1)}) %all-gather.4.cloned.1.call-update) | async-done | bytes 3145744 | tf_op jit(solution)/shard_map/all_gather | solution.py:110
  61.9 8.8 %fusion.44 = bf16[768,1536]{1,0:T(8,128)(2,1)S(1)} fusion(bf16[768,2048]{1,0:T(8,128)(2,1)} %all-gather.4.cloned.1.call-done, bf16[2048,512]{1,0:T(8,128)(2,1)} %param.25, bf16[2048,512]{1,0:T(8,128)(2,1)} %param.24, bf16[2048,512]{1,0:T(8,128)(2,1)} %param.23), kind=kOutput, calls=%fused_computation.56 | convolution fusion | flops 4851892224 | bytes 11796480 | tf_op jit(solution)/shard_map/dot_general | solution.py:109
  73.9 39.3 %all-gather.6.cloned.1.call-done = bf16[1024,1024]{1,0:T(8,128)(2,1)} async-done(((bf16[128,1024]{1,0:T(8,128)(2,1)}), bf16[1024,1024]{1,0:T(8,128)(2,1)}) %all-gather.6.cloned.1.call-update) | async-done | bytes 2097168 | tf_op jit(solution)/shard_map/all_gather | solution.py:127
  124.0 3.1 fusion.67
  127.1 6.2 %fusion.25 = (f32[4,768]{1,0:T(4,128)S(1)}, f32[4,768]{1,0:T(4,128)S(1)}, f32[4,768,1024]{2,1,0:T(8,128)}) fusion(f32[4]{0:T(128)S(1)} %copy-done.9, f32[4,768,1024]{2,1,0:T(8,128)S(1)} %fusion.67, bf16[1024,4,2,64]{0,3,2,1:T(8,128)(2,1)S(1)} %bitcast.155, bf16[768,4,2,64]{0,3,2,1:T(8,128)(2,1)S(1)} %bitcast.153), kind=kOutput, calls=%fused_computation.39 | convolution fusion | flops 421521408 | bytes 26108416 | tf_op jit(solution)/shard_map/qhd,khd->hqk/dot_general | solution.py:35
  133.3 8.2 %fusion.29 = (f32[4,768]{1,0:T(4,128)S(1)}, f32[4,768]{1,0:T(4,128)S(1)}) fusion(f32[4,768,1024]{2,1,0:T(8,128)} %get-tuple-element.134, f32[4,768]{1,0:T(4,128)S(1)} %broadcast_maximum_fusion, f32[4]{0:T(128)S(1)} %copy-done.9, f32[4,768]{1,0:T(4,128)S(1)} %broadcast_maximum_fusion.1, f32[4,768,1024]{2,1,0:T(8,128)S(1)} %fusion.67), kind=kLoop, calls=%fused_computation.43 | loop fusion | flops 25159680 | bytes 25214992 | tf_op jit(solution)/shard_map/reduce_sum | solution.py:47
  141.5 8.6 %bitcast_add_fusion.2 = f32[768,4,128]{0,2,1:T(8,128)} fusion(bf16[1024,4,128]{0,2,1:T(8,128)(2,1)S(1)} %bitcast.156, f32[4,768,1024]{2,1,0:T(8,128)} %get-tuple-element.134, f32[4,768]{1,0:T(4,128)S(1)} %broadcast_maximum_fusion, f32[4]{0:T(128)S(1)} %copy-done.9, f32[768,4]{0,1:T(4,128)S(1)} %get-tuple-element.136), kind=kOutput, calls=%fused_computation.67 | convolution fusion | flops 818282496 | bytes 15228944 | tf_op jit(solution)/shard_map/hqk,khd->qhd/dot_general | solution.py:48
  150.1 4.1 bitcast_add_fusion.3
  154.2 135.8 %all-gather.8.cloned.1.call-done = bf16[6144,1024]{1,0:T(8,128)(2,1)} async-done(((bf16[768,1024]{1,0:T(8,128)(2,1)}), bf16[6144,1024]{1,0:T(8,128)(2,1)}) %all-gather.8.cloned.1.call-update) | async-done | bytes 12582928 | tf_op jit(solution)/shard_map/all_gather | solution.py:135
  290.0 193.8 %while.20 = (s32[]{:T(128)}, f32[4,768]{1,0:T(4,128)S(1)}, f32[4,768]{1,0:T(4,128)S(1)}, f32[768,4,128]{0,2,1:T(8,128)}, f32[4,768]{1,0:T(4,128)S(1)}, /*index=5...) while((s32[]{:T(128)}, f32[4,768]{1,0:T(4,128)S(1)}, ...), condition=%wide.region_11.12_spmd, body=%wide.region_6.11_spmd.sunk | while | flops 2486716416 | bytes 128058136 | solution.py:69
  290.0 3.1 constant_dynamic-slice_fusion.2
  293.1 3.9 copy.54
  297.1 2.7 fusion.116
  299.8 2.8 fusion.117
  302.6 5.5 %bitcast_reduce_fusion.3 = (f32[4,768]{1,0:T(4,128)S(1)}, f32[4,768]{1,0:T(4,128)S(1)}, f32[4,1024,768]{2,1,0:T(8,128)S(1)}) fusion(f32[4]{0:T(128)S(1)} %broadcast_multiply_fusion.2, f32[4,1024,768]{2,1,0:T(8,128)S(1)} %fusion.117, bf16[768,4,2,64]{0,3,1,2:T(8,128)(2,1)} %get-tuple-element.254, bf16[1024,4,2,64]{0,3,2,1:T(8,128)(2,1)S(1)} %bitcast.147), kind=kOutput, calls=%fused_computation.1.clone.1 | convolution fusion | flops 421521408 | bytes 26108416 | tf_op jit(solution)/shard_map/while/body/eval_jaxpr/qhd,khd->hqk/dot_general | solution.py:35
  308.1 5.8 %bitcast_add_fusion.7 = f32[768,4,128]{0,2,1:T(8,128)} fusion(f32[768,4,128]{0,2,1:T(8,128)} %get-tuple-element.241, bf16[1024,4,128]{0,2,1:T(8,128)(2,1)} %bitcast.148, f32[4,1024,768]{2,1,0:T(8,128)S(1)} %get-tuple-element.214, f32[4,768]{1,0:T(4,128)S(1)} %get-tuple-element.250, f32[4]{0:T(128)S(1)} %broadcast_multiply_fusion.2, ...), kind=kOutput, calls=%fused_computation.14.clone.1 | convolution fusion | flops 818675712 | bytes 16801808 | tf_op jit(solution)/shard_map/while/body/eval_jaxpr/hqk,khd->qhd/dot_general | solution.py:48
  313.9 3.2 bitcast_add_fusion.6
  317.1 5.1 fusion.120
  322.4 3.1 constant_dynamic-slice_fusion.2
  325.4 3.9 copy.54
  329.4 2.7 fusion.116
  332.1 2.8 fusion.117
  334.9 5.5 %bitcast_reduce_fusion.3 = (f32[4,768]{1,0:T(4,128)S(1)}, f32[4,768]{1,0:T(4,128)S(1)}, f32[4,1024,768]{2,1,0:T(8,128)S(1)}) fusion(f32[4]{0:T(128)S(1)} %broadcast_multiply_fusion.2, f32[4,1024,768]{2,1,0:T(8,128)S(1)} %fusion.117, bf16[768,4,2,64]{0,3,1,2:T(8,128)(2,1)} %get-tuple-element.254, bf16[1024,4,2,64]{0,3,2,1:T(8,128)(2,1)S(1)} %bitcast.147), kind=kOutput, calls=%fused_computation.1.clone.1 | convolution fusion | flops 421521408 | bytes 26108416 | tf_op jit(solution)/shard_map/while/body/eval_jaxpr/qhd,khd->hqk/dot_general | solution.py:35
  340.4 5.8 %bitcast_add_fusion.7 = f32[768,4,128]{0,2,1:T(8,128)} fusion(f32[768,4,128]{0,2,1:T(8,128)} %get-tuple-element.241, bf16[1024,4,128]{0,2,1:T(8,128)(2,1)} %bitcast.148, f32[4,1024,768]{2,1,0:T(8,128)S(1)} %get-tuple-element.214, f32[4,768]{1,0:T(4,128)S(1)} %get-tuple-element.250, f32[4]{0:T(128)S(1)} %broadcast_multiply_fusion.2, ...), kind=kOutput, calls=%fused_computation.14.clone.1 | convolution fusion | flops 818675712 | bytes 16801808 | tf_op jit(solution)/shard_map/while/body/eval_jaxpr/hqk,khd->qhd/dot_general | solution.py:48
  346.2 3.2 bitcast_add_fusion.6
  349.4 5.1 fusion.120
  354.7 3.1 constant_dynamic-slice_fusion.2
  357.7 3.9 copy.54
  361.7 2.7 fusion.116
  364.4 2.8 fusion.117
  367.2 5.5 %bitcast_reduce_fusion.3 = (f32[4,768]{1,0:T(4,128)S(1)}, f32[4,768]{1,0:T(4,128)S(1)}, f32[4,1024,768]{2,1,0:T(8,128)S(1)}) fusion(f32[4]{0:T(128)S(1)} %broadcast_multiply_fusion.2, f32[4,1024,768]{2,1,0:T(8,128)S(1)} %fusion.117, bf16[768,4,2,64]{0,3,1,2:T(8,128)(2,1)} %get-tuple-element.254, bf16[1024,4,2,64]{0,3,2,1:T(8,128)(2,1)S(1)} %bitcast.147), kind=kOutput, calls=%fused_computation.1.clone.1 | convolution fusion | flops 421521408 | bytes 26108416 | tf_op jit(solution)/shard_map/while/body/eval_jaxpr/qhd,khd->hqk/dot_general | solution.py:35
  372.7 5.8 %bitcast_add_fusion.7 = f32[768,4,128]{0,2,1:T(8,128)} fusion(f32[768,4,128]{0,2,1:T(8,128)} %get-tuple-element.241, bf16[1024,4,128]{0,2,1:T(8,128)(2,1)} %bitcast.148, f32[4,1024,768]{2,1,0:T(8,128)S(1)} %get-tuple-element.214, f32[4,768]{1,0:T(4,128)S(1)} %get-tuple-element.250, f32[4]{0:T(128)S(1)} %broadcast_multiply_fusion.2, ...), kind=kOutput, calls=%fused_computation.14.clone.1 | convolution fusion | flops 818675712 | bytes 16801808 | tf_op jit(solution)/shard_map/while/body/eval_jaxpr/hqk,khd->qhd/dot_general | solution.py:48
  378.5 3.2 bitcast_add_fusion.6
  381.7 5.1 fusion.120
  387.0 3.1 constant_dynamic-slice_fusion.2
  390.0 3.9 copy.54
  394.0 2.7 fusion.116
  396.7 2.8 fusion.117
  399.5 5.5 %bitcast_reduce_fusion.3 = (f32[4,768]{1,0:T(4,128)S(1)}, f32[4,768]{1,0:T(4,128)S(1)}, f32[4,1024,768]{2,1,0:T(8,128)S(1)}) fusion(f32[4]{0:T(128)S(1)} %broadcast_multiply_fusion.2, f32[4,1024,768]{2,1,0:T(8,128)S(1)} %fusion.117, bf16[768,4,2,64]{0,3,1,2:T(8,128)(2,1)} %get-tuple-element.254, bf16[1024,4,2,64]{0,3,2,1:T(8,128)(2,1)S(1)} %bitcast.147), kind=kOutput, calls=%fused_computation.1.clone.1 | convolution fusion | flops 421521408 | bytes 26108416 | tf_op jit(solution)/shard_map/while/body/eval_jaxpr/qhd,khd->hqk/dot_general | solution.py:35
  405.0 5.8 %bitcast_add_fusion.7 = f32[768,4,128]{0,2,1:T(8,128)} fusion(f32[768,4,128]{0,2,1:T(8,128)} %get-tuple-element.241, bf16[1024,4,128]{0,2,1:T(8,128)(2,1)} %bitcast.148, f32[4,1024,768]{2,1,0:T(8,128)S(1)} %get-tuple-element.214, f32[4,768]{1,0:T(4,128)S(1)} %get-tuple-element.250, f32[4]{0:T(128)S(1)} %broadcast_multiply_fusion.2, ...), kind=kOutput, calls=%fused_computation.14.clone.1 | convolution fusion | flops 818675712 | bytes 16801808 | tf_op jit(solution)/shard_map/while/body/eval_jaxpr/hqk,khd->qhd/dot_general | solution.py:48
  410.8 3.2 bitcast_add_fusion.6
  414.0 5.1 fusion.120
  419.3 3.1 constant_dynamic-slice_fusion.2
  422.3 3.9 copy.54
  426.3 2.7 fusion.116
  429.0 2.8 fusion.117
  431.8 5.5 %bitcast_reduce_fusion.3 = (f32[4,768]{1,0:T(4,128)S(1)}, f32[4,768]{1,0:T(4,128)S(1)}, f32[4,1024,768]{2,1,0:T(8,128)S(1)}) fusion(f32[4]{0:T(128)S(1)} %broadcast_multiply_fusion.2, f32[4,1024,768]{2,1,0:T(8,128)S(1)} %fusion.117, bf16[768,4,2,64]{0,3,1,2:T(8,128)(2,1)} %get-tuple-element.254, bf16[1024,4,2,64]{0,3,2,1:T(8,128)(2,1)S(1)} %bitcast.147), kind=kOutput, calls=%fused_computation.1.clone.1 | convolution fusion | flops 421521408 | bytes 26108416 | tf_op jit(solution)/shard_map/while/body/eval_jaxpr/qhd,khd->hqk/dot_general | solution.py:35
  437.3 5.8 %bitcast_add_fusion.7 = f32[768,4,128]{0,2,1:T(8,128)} fusion(f32[768,4,128]{0,2,1:T(8,128)} %get-tuple-element.241, bf16[1024,4,128]{0,2,1:T(8,128)(2,1)} %bitcast.148, f32[4,1024,768]{2,1,0:T(8,128)S(1)} %get-tuple-element.214, f32[4,768]{1,0:T(4,128)S(1)} %get-tuple-element.250, f32[4]{0:T(128)S(1)} %broadcast_multiply_fusion.2, ...), kind=kOutput, calls=%fused_computation.14.clone.1 | convolution fusion | flops 818675712 | bytes 16801808 | tf_op jit(solution)/shard_map/while/body/eval_jaxpr/hqk,khd->qhd/dot_general | solution.py:48
  443.1 3.2 bitcast_add_fusion.6
  446.3 5.1 fusion.120
  451.6 3.1 constant_dynamic-slice_fusion.2
  454.6 3.9 copy.54
  458.6 2.7 fusion.116
  461.3 2.8 fusion.117
  464.1 5.5 %bitcast_reduce_fusion.3 = (f32[4,768]{1,0:T(4,128)S(1)}, f32[4,768]{1,0:T(4,128)S(1)}, f32[4,1024,768]{2,1,0:T(8,128)S(1)}) fusion(f32[4]{0:T(128)S(1)} %broadcast_multiply_fusion.2, f32[4,1024,768]{2,1,0:T(8,128)S(1)} %fusion.117, bf16[768,4,2,64]{0,3,1,2:T(8,128)(2,1)} %get-tuple-element.254, bf16[1024,4,2,64]{0,3,2,1:T(8,128)(2,1)S(1)} %bitcast.147), kind=kOutput, calls=%fused_computation.1.clone.1 | convolution fusion | flops 421521408 | bytes 26108416 | tf_op jit(solution)/shard_map/while/body/eval_jaxpr/qhd,khd->hqk/dot_general | solution.py:35
  469.6 5.8 %bitcast_add_fusion.7 = f32[768,4,128]{0,2,1:T(8,128)} fusion(f32[768,4,128]{0,2,1:T(8,128)} %get-tuple-element.241, bf16[1024,4,128]{0,2,1:T(8,128)(2,1)} %bitcast.148, f32[4,1024,768]{2,1,0:T(8,128)S(1)} %get-tuple-element.214, f32[4,768]{1,0:T(4,128)S(1)} %get-tuple-element.250, f32[4]{0:T(128)S(1)} %broadcast_multiply_fusion.2, ...), kind=kOutput, calls=%fused_computation.14.clone.1 | convolution fusion | flops 818675712 | bytes 16801808 | tf_op jit(solution)/shard_map/while/body/eval_jaxpr/hqk,khd->qhd/dot_general | solution.py:48
  475.4 3.2 bitcast_add_fusion.6
  478.6 5.1 fusion.120
  486.5 3.5 convolution_convert_fusion
  490.0 36.2 %reduce-scatter.2.cloned.1.call-done = bf16[192,2048]{1,0:T(8,128)(2,1)} async-done(((bf16[768,2048]{1,0:T(8,128)(2,1)}), bf16[192,2048]{1,0:T(8,128)(2,1)}) %reduce-scatter.2.cloned.1.call-update) | async-done | bytes 786448 | tf_op jit(solution)/shard_map/reduce_scatter | solution.py:145
  (129 shorter events, 34.4 us)
Async XLA Ops:
  6.5 480.0 %copy-start = (bf16[512,2048]{1,0:T(8,128)(2,1)S(1)}, bf16[512,2048]{1,0:T(8,128)(2,1)}, u32[]{:S(2)}) copy-start(bf16[512,2048]{1,0:T(8,128)(2,1)} %param.26) | copy-start | bytes 6291460
  6.5 55.4 %all-gather.4.cloned.1.call-start = ((), (), s32[]{:S(2)}) async-start(), calls=%async_computation.1 | async-start | bytes 3932160 | tf_op jit(solution)/shard_map/all_gather | solution.py:110
  10.0 4.7 collective-permute-start
  14.8 3.8 collective-permute-start.1
  18.6 4.8 collective-permute-start.2
  31.7 81.5 %all-gather.6.cloned.1.call-start = ((), (), s32[]{:S(2)}) async-start(), calls=%async_computation.2 | async-start | bytes 2359296 | tf_op jit(solution)/shard_map/all_gather | solution.py:127
  36.9 253.2 %all-gather.8.cloned.1.call-start = ((), (), s32[]{:S(2)}) async-start(), calls=%async_computation.3 | async-start | bytes 14155776 | tf_op jit(solution)/shard_map/all_gather | solution.py:135
  70.7 1.4 copy-start.4
  73.6 452.6 %reduce-scatter.2.cloned.1.call-start = ((), (), s32[]{:S(2)}) async-start(), calls=%async_computation.4 | async-start | bytes 3932160 | tf_op jit(solution)/shard_map/reduce_scatter | solution.py:145
  124.0 3.1 copy-start.3
  124.0 3.1 copy-start.9
  133.3 8.2 %copy-start.7 = (bf16[1024,512]{0,1:T(8,128)(2,1)S(1)}, bf16[1024,512]{0,1:T(8,128)(2,1)}, u32[]{:S(2)}) copy-start(bf16[1024,512]{0,1:T(8,128)(2,1)} %copy.41) | copy-start | bytes 3145732
  290.0 193.8 %copy-start.10 = (f32[4]{0:T(128)S(1)}, f32[4]{0:T(128)}, u32[]{:S(2)}) copy-start(f32[4]{0:T(128)} %param.27) | copy-start | bytes 52
  290.0 196.1 %copy-start.11 = (f32[128]{0:T(128)S(1)}, f32[128]{0:T(128)}, u32[]{:S(2)}) copy-start(f32[128]{0:T(128)} %param.29) | copy-start | bytes 1540
  308.1 5.8 %copy-start.1 = (bf16[1024,512]{0,1:T(8,128)(2,1)S(1)}, bf16[1024,512]{0,1:T(8,128)(2,1)}, u32[]{:S(2)}) copy-start(bf16[1024,512]{0,1:T(8,128)(2,1)} %get-tuple-element.220) | copy-start | bytes 3145732 | tf_op jit(solution)/shard_map/while
  308.1 5.8 %copy-start.5 = (f32[768,4,128]{0,2,1:T(8,128)S(1)}, f32[768,4,128]{0,2,1:T(8,128)}, u32[]{:S(2)}) copy-start(f32[768,4,128]{0,2,1:T(8,128)} %get-tuple-element.238) | copy-start | bytes 4718596 | tf_op jit(solution)/shard_map/while
  317.1 5.2 copy-start.6
  340.4 5.8 %copy-start.1 = (bf16[1024,512]{0,1:T(8,128)(2,1)S(1)}, bf16[1024,512]{0,1:T(8,128)(2,1)}, u32[]{:S(2)}) copy-start(bf16[1024,512]{0,1:T(8,128)(2,1)} %get-tuple-element.220) | copy-start | bytes 3145732 | tf_op jit(solution)/shard_map/while
  340.4 5.8 %copy-start.5 = (f32[768,4,128]{0,2,1:T(8,128)S(1)}, f32[768,4,128]{0,2,1:T(8,128)}, u32[]{:S(2)}) copy-start(f32[768,4,128]{0,2,1:T(8,128)} %get-tuple-element.238) | copy-start | bytes 4718596 | tf_op jit(solution)/shard_map/while
  349.4 5.2 copy-start.6
  372.7 5.8 %copy-start.1 = (bf16[1024,512]{0,1:T(8,128)(2,1)S(1)}, bf16[1024,512]{0,1:T(8,128)(2,1)}, u32[]{:S(2)}) copy-start(bf16[1024,512]{0,1:T(8,128)(2,1)} %get-tuple-element.220) | copy-start | bytes 3145732 | tf_op jit(solution)/shard_map/while
  372.7 5.8 %copy-start.5 = (f32[768,4,128]{0,2,1:T(8,128)S(1)}, f32[768,4,128]{0,2,1:T(8,128)}, u32[]{:S(2)}) copy-start(f32[768,4,128]{0,2,1:T(8,128)} %get-tuple-element.238) | copy-start | bytes 4718596 | tf_op jit(solution)/shard_map/while
  381.7 5.2 copy-start.6
  405.0 5.8 %copy-start.1 = (bf16[1024,512]{0,1:T(8,128)(2,1)S(1)}, bf16[1024,512]{0,1:T(8,128)(2,1)}, u32[]{:S(2)}) copy-start(bf16[1024,512]{0,1:T(8,128)(2,1)} %get-tuple-element.220) | copy-start | bytes 3145732 | tf_op jit(solution)/shard_map/while
  405.0 5.8 %copy-start.5 = (f32[768,4,128]{0,2,1:T(8,128)S(1)}, f32[768,4,128]{0,2,1:T(8,128)}, u32[]{:S(2)}) copy-start(f32[768,4,128]{0,2,1:T(8,128)} %get-tuple-element.238) | copy-start | bytes 4718596 | tf_op jit(solution)/shard_map/while
  414.0 5.2 copy-start.6
  437.3 5.8 %copy-start.1 = (bf16[1024,512]{0,1:T(8,128)(2,1)S(1)}, bf16[1024,512]{0,1:T(8,128)(2,1)}, u32[]{:S(2)}) copy-start(bf16[1024,512]{0,1:T(8,128)(2,1)} %get-tuple-element.220) | copy-start | bytes 3145732 | tf_op jit(solution)/shard_map/while
  437.3 5.8 %copy-start.5 = (f32[768,4,128]{0,2,1:T(8,128)S(1)}, f32[768,4,128]{0,2,1:T(8,128)}, u32[]{:S(2)}) copy-start(f32[768,4,128]{0,2,1:T(8,128)} %get-tuple-element.238) | copy-start | bytes 4718596 | tf_op jit(solution)/shard_map/while
  446.3 5.2 copy-start.6
  469.6 5.8 %copy-start.1 = (bf16[1024,512]{0,1:T(8,128)(2,1)S(1)}, bf16[1024,512]{0,1:T(8,128)(2,1)}, u32[]{:S(2)}) copy-start(bf16[1024,512]{0,1:T(8,128)(2,1)} %get-tuple-element.220) | copy-start | bytes 3145732 | tf_op jit(solution)/shard_map/while
  469.6 5.8 %copy-start.5 = (f32[768,4,128]{0,2,1:T(8,128)S(1)}, f32[768,4,128]{0,2,1:T(8,128)}, u32[]{:S(2)}) copy-start(f32[768,4,128]{0,2,1:T(8,128)} %get-tuple-element.238) | copy-start | bytes 4718596 | tf_op jit(solution)/shard_map/while
  478.6 5.2 copy-start.6
  486.5 39.8 %copy-start.2 = (bf16[192,2048]{1,0:T(8,128)(2,1)S(1)}, bf16[192,2048]{1,0:T(8,128)(2,1)}, u32[]{:S(2)}) copy-start(bf16[192,2048]{1,0:T(8,128)(2,1)} %param.16) | copy-start | bytes 2359300
  486.5 39.7 %copy-start.8 = (f32[1,1,2048]{2,0,1:T(1,128)S(1)}, f32[1,1,2048]{2,0,1:T(1,128)}, u32[]{:S(2)}) copy-start(f32[1,1,2048]{2,0,1:T(1,128)} %get-tuple-element.125) | copy-start | bytes 24580
Sparse Core Ops, SparseCore 0:
  31.8 30.0 all-gather.3
  64.0 49.0 all-gather.5
  115.4 174.6 all-gather.7
  490.1 36.0 reduce-scatter.1
